TPU v7x, 32 devices: a whole 2x2x4 slice. The times are simulated.
32 devices in a mesh: sp: 8 (over z, y), tp: 4 (over x, core).
Axes of the slice: x: 2, y: 2, z: 4, core: 2. Of those that a mesh axis runs over, the one named last changes fastest.
Arguments:
- resid: bfloat16 [3072, 2048], P('sp', 'tp'), may hold values from -6 to 6
- mixer_in: bfloat16 [3072, 2048], P('sp', 'tp'), may hold values from -6 to 6
- log_step: float32 [3072, 128], P('sp', 'tp'), may hold values from -5.2 to -0.79
- decay_real: float32 [128, 64], P('tp'), may hold values from 0.00016276042 to 0.8
- frequency: float32 [128, 64], P('tp'), may hold values from 0.5 to 6
- input_matrix: float32 [2, 128, 64, 16], P(None, 'tp'), may hold values from -1 to 1
- output_matrix: float32 [2, 128, 16, 64], P(None, 'tp'), may hold values from -0.5 to 0.5
- skip_gain: float32 [2048], P('tp'), may hold values from -4 to 4
- value_weight: bfloat16 [2048, 2048], P(None, 'tp'), may hold values from -0.125 to 0.125
- gate_weight: bfloat16 [2048, 2048], P(None, 'tp'), may hold values from -0.125 to 0.125
- norm_gain: float32 [2048], replicated, may hold values from 0.1 to 1.9
- up_weight: bfloat16 [2048, 8192], P('sp', 'tp'), may hold values from -0.125 to 0.125
- down_weight: bfloat16 [2048, 8192], P('sp', 'tp'), may hold values from -0.0625 to 0.0625
Outputs:
- result: bfloat16 [3072, 2048], P('sp', 'tp')
All inputs are finite; a program needn't handle non-finite values.
Results may differ from a plain program's by a relative error of at most 0.014.
Values may be sent and summed in bfloat16 or wider, within the bound.
A program may use at most 128 MiB of HBM per device.

v0:
```python
import jax
import jax.numpy as jnp
from jax import lax
from jax.sharding import PartitionSpec as P

rms_eps = 1e-06
highest = lax.Precision.HIGHEST


def prefix(part, axis, combine, identity):
    place = lax.axis_index(axis)
    gathered = jax.tree.map(lambda a: lax.all_gather(a, axis), part)
    state = jax.tree.map(lambda a, e: jnp.zeros_like(a) + jnp.asarray(e, a.dtype), part, identity)

    def one(step, state):
        return combine(
            state, jax.tree.map(lambda a: lax.dynamic_index_in_dim(a, step, 0, False), gathered)
        )

    return lax.fori_loop(0, place, one, state)


def chain_link(earlier, later):
    return (
        earlier[0] * later[0] - earlier[1] * later[1],
        earlier[0] * later[1] + earlier[1] * later[0],
        later[0] * earlier[2] - later[1] * earlier[3] + later[2],
        later[0] * earlier[3] + later[1] * earlier[2] + later[3],
    )


def discretize(log_step, decay_real, frequency):
    states = decay_real.shape[1]
    step_size = jnp.repeat(jnp.exp(log_step), states, axis=1)
    decay_rate = decay_real.reshape(-1)
    angular = frequency.reshape(-1)
    shrink = -decay_rate * step_size
    rotation = angular * step_size
    factor = jnp.exp(shrink)
    decay_re = factor * jnp.cos(rotation)
    decay_im = factor * jnp.sin(rotation)
    half_sine = jnp.sin(0.5 * rotation)
    minus_re = jnp.expm1(shrink) * jnp.cos(rotation) - 2.0 * half_sine * half_sine
    modulus = decay_rate * decay_rate + angular * angular
    drive_re = (decay_im * angular - minus_re * decay_rate) / modulus
    drive_im = (-decay_im * decay_rate - minus_re * angular) / modulus
    return (decay_re, decay_im, drive_re, drive_im)


def local_states(mixer_in, log_step, decay_real, frequency, input_matrix):
    tokens = mixer_in.shape[0]
    groups, states = decay_real.shape
    signal = mixer_in.astype(jnp.float32).reshape(tokens, groups, -1)
    proj_re = jnp.einsum("tgk,gnk->tgn", signal, input_matrix[0], precision=highest).reshape(
        tokens, groups * states
    )
    proj_im = jnp.einsum("tgk,gnk->tgn", signal, input_matrix[1], precision=highest).reshape(
        tokens, groups * states
    )
    decay_re, decay_im, drive_re, drive_im = discretize(log_step, decay_real, frequency)
    feed_re = drive_re * proj_re - drive_im * proj_im
    feed_im = drive_re * proj_im + drive_im * proj_re
    chain_rows = lax.associative_scan(chain_link, (decay_re, decay_im, feed_re, feed_im), axis=0)
    end_states = tuple((member[-1] for member in chain_rows))
    return (end_states, chain_rows)


def read_out(state_re, state_im, output_matrix):
    tokens = state_re.shape[0]
    groups = output_matrix.shape[1]
    grid_re = state_re.reshape(tokens, groups, -1)
    grid_im = state_im.reshape(tokens, groups, -1)
    output = jnp.einsum("tgn,gkn->tgk", grid_re, output_matrix[0], precision=highest)
    output = output - jnp.einsum("tgn,gkn->tgk", grid_im, output_matrix[1], precision=highest)
    return output.reshape(tokens, -1)


def per_device(
    resid,
    mixer_in,
    log_step,
    decay_real,
    frequency,
    input_matrix,
    output_matrix,
    skip_gain,
    value_weight,
    gate_weight,
    norm_gain,
    up_weight,
    down_weight,
):
    end_states, chain_rows = local_states(mixer_in, log_step, decay_real, frequency, input_matrix)
    cum_re, cum_im, part_re, part_im = chain_rows
    zero_state = jnp.zeros_like(end_states[0])
    identity_state = (jnp.ones_like(end_states[0]), zero_state, zero_state, zero_state)
    _, _, carry_re, carry_im = prefix(end_states, "sp", chain_link, identity_state)
    state_re = part_re + cum_re * carry_re - cum_im * carry_im
    state_im = part_im + cum_re * carry_im + cum_im * carry_re
    mechanism = read_out(state_re, state_im, output_matrix) + skip_gain * mixer_in.astype(
        jnp.float32
    )
    mixed_out = jax.nn.gelu(mechanism).astype(jnp.bfloat16)
    channels = lax.all_gather(mixed_out, "tp", axis=1, tiled=True)
    value_pre = jnp.dot(channels, value_weight, preferred_element_type=jnp.float32)
    gate_pre = jnp.dot(channels, gate_weight, preferred_element_type=jnp.float32)
    updated = (resid.astype(jnp.float32) + value_pre * jax.nn.sigmoid(gate_pre)).astype(
        jnp.bfloat16
    )
    updated_wide = lax.optimization_barrier(updated).astype(jnp.float32)
    whole_rows = lax.all_gather(updated, "tp", axis=1, tiled=True).astype(jnp.float32)
    inv_rms = lax.rsqrt(jnp.mean(whole_rows * whole_rows, axis=1, keepdims=True) + rms_eps)
    normed = (whole_rows * inv_rms * norm_gain).astype(jnp.bfloat16)
    raised = jnp.dot(
        normed,
        lax.all_gather(up_weight, "sp", axis=0, tiled=True),
        preferred_element_type=jnp.float32,
    )
    active = jax.nn.relu(raised)
    hidden = (active * active).astype(jnp.bfloat16)
    partials = lax.dot_general(
        hidden,
        lax.all_gather(down_weight, "sp", axis=0, tiled=True),
        (((1,), (1,)), ((), ())),
        preferred_element_type=jnp.float32,
    )
    down_sum = lax.psum_scatter(
        partials.astype(jnp.bfloat16), "tp", scatter_dimension=1, tiled=True
    ).astype(jnp.float32)
    return (updated_wide + down_sum).astype(jnp.bfloat16)


def solution(mesh):
    in_specs = (
        P("sp", "tp"),
        P("sp", "tp"),
        P("sp", "tp"),
        P("tp", None),
        P("tp", None),
        P(None, "tp", None, None),
        P(None, "tp", None, None),
        P("tp"),
        P(None, "tp"),
        P(None, "tp"),
        P(),
        P("sp", "tp"),
        P("sp", "tp"),
    )
    out_specs = P("sp", "tp")
    return jax.shard_map(
        per_device, mesh=mesh, in_specs=in_specs, out_specs=out_specs, check_vma=False
    )
```

profile of v0, /device:TPU:0, one launch (start us, length us, event | category | flops | bytes accessed | tf_op | source)
XLA Modules:
  0.0 1072.0 jit_solution(13489932872210937987)
XLA Ops:
  28.5 27.8 %multiply_add_fusion.1 = (f32[384,2048]{1,0:T(8,128)}, f32[384,2048]{1,0:T(8,128)}, f32[384,2048]{1,0:T(8,128)}, f32[384,2048]{1,0:T(8,128)}) fusion(f32[384,2048]{1,0:T(8,128)} %copy.169, f32[384,2048]{1,0:T(8,128)} %copy.170, f32[2048]{0:T(1024)S(1)} %get-tuple-element.187, f32[2048]{0:T(1024)S(1)} %reshape.55, f32[384,2048]{1,0:T(8,128)} %copy.166, ...), kind=kLoop, calls=%fused_computation.16 | loop fusion | flops 18874368 | bytes 22052864 | tf_op jit(solution)/shard_map/add | solution.py:62
  56.3 7.6 slice.501
  63.9 7.6 slice.504
  71.5 7.6 slice.500
  79.1 7.6 slice.506
  86.7 7.6 slice.502
  94.3 7.6 slice.507
  101.8 7.6 slice.503
  109.4 7.6 slice.512
  117.0 9.2 multiply_subtract_fusion.3
  126.3 4.3 slice.510
  135.0 4.3 slice.509
  143.6 4.3 slice.511
  148.0 4.4 slice.517
  156.6 4.3 slice.522
  161.0 4.9 add_add_fusion.4
  283.2 4.4 slice.508
  287.6 4.4 slice.607
  292.0 4.4 slice.611
  296.4 4.4 slice.615
  303.7 7.8 slice.499
  311.5 7.8 slice.613
  319.3 7.8 slice.617
  327.1 8.0 slice.652
  425.8 5.1 pad.223
  434.3 9.6 pad.259
  448.5 5.1 pad.221
  460.2 5.1 pad.253
  465.3 5.2 pad.251
  471.5 5.1 pad.250
  491.9 9.7 pad.258
  502.5 32.4 %all-gather.3 = f32[8,1,2048]{2,1,0:T(1,128)S(1)} all-gather(f32[1,1,2048]{2,1,0:T(1,128)S(1)} %add_bitcast_fusion), channel_id=1, replica_groups=mesh['sp'=8,'tp'=4] {'sp'}, dimensions={0}, use_global_device_ids=true | all-gather | bytes 73728 | tf_op jit(solution)/shard_map/all_gather | solution.py:12
  534.9 9.6 pad.225
  547.2 9.7 pad.224
  557.8 30.5 %all-gather.2 = f32[8,1,2048]{2,1,0:T(1,128)S(1)} all-gather(f32[1,1,2048]{2,1,0:T(1,128)S(1)} %add_bitcast_fusion.1), channel_id=1, replica_groups=mesh['sp'=8,'tp'=4] {'sp'}, dimensions={0}, use_global_device_ids=true | all-gather | bytes 73728 | tf_op jit(solution)/shard_map/all_gather | solution.py:12
  591.1 9.8 pad.256
  600.9 9.6 pad.257
  611.4 30.5 %all-gather.1 = f32[8,1,2048]{2,1,0:T(1,128)S(1)} all-gather(f32[1,1,2048]{2,1,0:T(1,128)S(1)} %add_bitcast_fusion.2), channel_id=1, replica_groups=mesh['sp'=8,'tp'=4] {'sp'}, dimensions={0}, use_global_device_ids=true | all-gather | bytes 73728 | tf_op jit(solution)/shard_map/all_gather | solution.py:12
  644.8 9.7 pad.254
  654.4 9.7 pad.255
  665.0 30.5 %all-gather = f32[8,1,2048]{2,1,0:T(1,128)S(1)} all-gather(f32[1,1,2048]{2,1,0:T(1,128)S(1)} %add_bitcast_fusion.3), channel_id=1, replica_groups=mesh['sp'=8,'tp'=4] {'sp'}, dimensions={0}, use_global_device_ids=true | all-gather | bytes 73728 | tf_op jit(solution)/shard_map/all_gather | solution.py:12
  695.6 13.3 %multiply_add_fusion = (f32[384,2048]{1,0:T(8,128)}, f32[384,2048]{1,0:T(8,128)}) fusion(f32[384,2048]{1,0:T(8,128)} %pad.258, f32[384,2048]{1,0:T(8,128)} %pad.259, f32[2048]{0:T(1024)S(1)} %get-tuple-element.76, f32[2048]{0:T(1024)S(1)} %get-tuple-element.75, f32[384,2048]{1,0:T(8,128)} %pad.256, f32[384,2048]{1,0:T(8,128)} %pad.257, ...), kind=kLoop, calls=%fused_computation.14 | loop fusion | flops 9437184 | bytes 31473664 | tf_op jit(solution)/shard_map/add | solution.py:99
  725.9 21.3 %all-gather.9.cloned.1.call-done = bf16[384,2048]{1,0:T(8,128)(2,1)} async-done(((bf16[384,512]{1,0:T(8,128)(2,1)}), bf16[384,2048]{1,0:T(8,128)(2,1)}) %all-gather.9.cloned.1.call-update) | async-done | bytes 1572880 | tf_op jit(solution)/shard_map/all_gather | solution.py:104
  753.3 18.1 %all-gather.11.cloned.1.call-done = bf16[384,2048]{1,0:T(8,128)(2,1)} async-done(((bf16[384,512]{1,0:T(8,128)(2,1)}), bf16[384,2048]{1,0:T(8,128)(2,1)}) %all-gather.11.cloned.1.call-update) | async-done | bytes 1572880 | tf_op jit(solution)/shard_map/all_gather | solution.py:111
  773.2 124.8 %all-gather.13.cloned.1.call-done = bf16[2048,2048]{1,0:T(8,128)(2,1)} async-done(((bf16[256,2048]{1,0:T(8,128)(2,1)}), bf16[2048,2048]{1,0:T(8,128)(2,1)}) %all-gather.13.cloned.1.call-update) | async-done | bytes 8388624 | tf_op jit(solution)/shard_map/all_gather | solution.py:116
  898.0 124.7 %all-gather.15.cloned.1.call-done = bf16[2048,2048]{1,0:T(8,128)(2,1)} async-done(((bf16[256,2048]{1,0:T(8,128)(2,1)}), bf16[2048,2048]{1,0:T(8,128)(2,1)}) %all-gather.15.cloned.1.call-update) | async-done | bytes 8388624 | tf_op jit(solution)/shard_map/all_gather | solution.py:123
  1022.7 14.1 %convolution_convert_fusion = bf16[384,2048]{1,0:T(8,128)(2,1)} fusion(bf16[2048,2048]{1,0:T(8,128)(2,1)} %all-gather.15.cloned.1.call-done, bf16[2048,2048]{1,0:T(8,128)(2,1)} %all-gather.13.cloned.1.call-done, bf16[384,2048]{1,0:T(8,128)(2,1)} %all-gather.11.cloned.1.call-done, f32[2048]{0:T(1024)S(1)} %copy-done.115, f32[384]{0:T(512)S(1)} %add_rsqrt_fusion), kind=kOutput, calls=%fused_computation.22 | convolution fusion | flops 6448742400 | bytes 19932672 | tf_op jit(solution)/shard_map/dot_general | solution.py:121
  1036.8 26.4 %reduce-scatter.2.cloned.1.call-done = bf16[384,512]{1,0:T(8,128)(2,1)} async-done(((bf16[384,2048]{1,0:T(8,128)(2,1)}), bf16[384,512]{1,0:T(8,128)(2,1)}) %reduce-scatter.2.cloned.1.call-update) | async-done | bytes 393232 | tf_op jit(solution)/shard_map/reduce_scatter | solution.py:127
  (491 shorter events, 313.9 us)
Async XLA Ops:
  6.5 740.6 %copy-start = (bf16[2048,512]{1,0:T(8,128)(2,1)S(1)}, bf16[2048,512]{1,0:T(8,128)(2,1)}, u32[]{:S(2)}) copy-start(bf16[2048,512]{1,0:T(8,128)(2,1)} %param.24) | copy-start | bytes 6291460
  6.5 740.6 %all-gather.9.cloned.1.call-start = ((), (), s32[]{:S(2)}) async-start(), calls=%async_computation.1 | async-start | bytes 1966080 | tf_op jit(solution)/shard_map/all_gather | solution.py:104
  7.9 4.2 copy-start.68
  228.7 15.8 %copy-start.69 = (f32[6,2048]{1,0:T(8,128)}, f32[6,2048]{1,0:T(8,128)S(1)}, u32[]{:S(2)}) copy-start(f32[6,2048]{1,0:T(8,128)S(1)} %get-tuple-element.173) | copy-start | bytes 147460
  327.0 27.7 %copy-start.73 = (f32[3,2048]{1,0:T(4,128)S(1)}, f32[3,2048]{1,0:T(4,128)}, u32[]{:S(2)}) copy-start(f32[3,2048]{1,0:T(4,128)} %slice.560) | copy-start | bytes 73732
  327.1 27.7 %copy-start.74 = (f32[3,2048]{1,0:T(4,128)S(1)}, f32[3,2048]{1,0:T(4,128)}, u32[]{:S(2)}) copy-start(f32[3,2048]{1,0:T(4,128)} %slice.564) | copy-start | bytes 73732
  327.1 27.7 %copy-start.75 = (f32[3,2048]{1,0:T(4,128)S(1)}, f32[3,2048]{1,0:T(4,128)}, u32[]{:S(2)}) copy-start(f32[3,2048]{1,0:T(4,128)} %slice.559) | copy-start | bytes 73732
  327.1 27.7 %copy-start.76 = (f32[3,2048]{1,0:T(4,128)S(1)}, f32[3,2048]{1,0:T(4,128)}, u32[]{:S(2)}) copy-start(f32[3,2048]{1,0:T(4,128)} %slice.566) | copy-start | bytes 73732
  327.1 27.7 %copy-start.77 = (f32[3,2048]{1,0:T(4,128)S(1)}, f32[3,2048]{1,0:T(4,128)}, u32[]{:S(2)}) copy-start(f32[3,2048]{1,0:T(4,128)} %slice.561) | copy-start | bytes 73732
  327.1 27.7 %copy-start.78 = (f32[3,2048]{1,0:T(4,128)S(1)}, f32[3,2048]{1,0:T(4,128)}, u32[]{:S(2)}) copy-start(f32[3,2048]{1,0:T(4,128)} %slice.567) | copy-start | bytes 73732
  327.1 27.7 %copy-start.79 = (f32[3,2048]{1,0:T(4,128)S(1)}, f32[3,2048]{1,0:T(4,128)}, u32[]{:S(2)}) copy-start(f32[3,2048]{1,0:T(4,128)} %slice.563) | copy-start | bytes 73732
  327.1 27.7 %copy-start.80 = (f32[3,2048]{1,0:T(4,128)S(1)}, f32[3,2048]{1,0:T(4,128)}, u32[]{:S(2)}) copy-start(f32[3,2048]{1,0:T(4,128)} %slice.571) | copy-start | bytes 73732
  335.1 20.4 %copy-start.72 = (f32[2,2048]{1,0:T(2,128)S(1)}, f32[2,2048]{1,0:T(2,128)}, u32[]{:S(2)}) copy-start(f32[2,2048]{1,0:T(2,128)} %slice.578) | copy-start | bytes 49156
  335.1 20.4 %copy-start.81 = (f32[2,2048]{1,0:T(2,128)S(1)}, f32[2,2048]{1,0:T(2,128)}, u32[]{:S(2)}) copy-start(f32[2,2048]{1,0:T(2,128)} %slice.581) | copy-start | bytes 49156
  335.1 20.4 %copy-start.82 = (f32[2,2048]{1,0:T(2,128)S(1)}, f32[2,2048]{1,0:T(2,128)}, u32[]{:S(2)}) copy-start(f32[2,2048]{1,0:T(2,128)} %slice.585) | copy-start | bytes 49156
  335.2 20.4 %copy-start.96 = (f32[1,2048]{1,0:T(1,128)S(1)}, f32[1,2048]{1,0:T(1,128)}, u32[]{:S(2)}) copy-start(f32[1,2048]{1,0:T(1,128)} %slice.662) | copy-start | bytes 24580
  335.2 20.4 %copy-start.97 = (f32[1,2048]{1,0:T(1,128)S(1)}, f32[1,2048]{1,0:T(1,128)}, u32[]{:S(2)}) copy-start(f32[1,2048]{1,0:T(1,128)} %slice.679) | copy-start | bytes 24580
  356.8 5.2 copy-start.54
  356.8 5.2 copy-start.55
  357.6 5.2 copy-start.66
  363.7 4.3 copy-start.65
  363.8 4.2 copy-start.104
  365.4 6.0 copy-start.40
  365.4 6.0 copy-start.41
  373.1 4.6 copy-start.29
  374.3 5.3 copy-start.31
  374.4 5.2 copy-start.33
  374.4 5.2 copy-start.101
  390.4 6.0 copy-start.92
  390.6 8.9 copy-start.17
  402.7 4.8 copy-start.48
  402.7 4.8 copy-start.94
  434.3 9.6 copy-start.88
  465.3 5.2 copy-start.36
  465.3 5.2 copy-start.90
  476.6 4.8 copy-start.6
  483.0 4.4 copy-start.24
  483.0 4.9 copy-start.25
  534.9 9.6 copy-start.84
  547.2 41.1 %copy-start.87 = (f32[1,2048]{1,0:T(1,128)S(1)}, f32[1,2048]{1,0:T(1,128)}, u32[]{:S(2)}) copy-start(f32[1,2048]{1,0:T(1,128)} %slice.752) | copy-start | bytes 24580
  600.9 41.1 %copy-start.85 = (f32[1,2048]{1,0:T(1,128)S(1)}, f32[1,2048]{1,0:T(1,128)}, u32[]{:S(2)}) copy-start(f32[1,2048]{1,0:T(1,128)} %slice.707) | copy-start | bytes 24580
  725.8 24.0 %copy-start.114 = (bf16[384,512]{1,0:T(8,128)(2,1)S(1)}, bf16[384,512]{1,0:T(8,128)(2,1)}, u32[]{:S(2)}) copy-start(bf16[384,512]{1,0:T(8,128)(2,1)} %param.15) | copy-start | bytes 1179652
  725.9 45.5 %all-gather.11.cloned.1.call-start = ((), (), s32[]{:S(2)}) async-start(), calls=%async_computation.2 | async-start | bytes 1966080 | tf_op jit(solution)/shard_map/all_gather | solution.py:111
  751.6 146.4 %all-gather.13.cloned.1.call-start = ((), (), s32[]{:S(2)}) async-start(), calls=%async_computation.3 | async-start | bytes 9437184 | tf_op jit(solution)/shard_map/all_gather | solution.py:116
  752.3 270.4 %copy-start.115 = (f32[2048]{0:T(1024)S(1)}, f32[2048]{0:T(1024)}, u32[]{:S(2)}) copy-start(f32[2048]{0:T(1024)} %param.25) | copy-start | bytes 24580
  752.3 270.3 %all-gather.15.cloned.1.call-start = ((), (), s32[]{:S(2)}) async-start(), calls=%async_computation.4 | async-start | bytes 9437184 | tf_op jit(solution)/shard_map/all_gather | solution.py:123
  752.9 310.2 %reduce-scatter.2.cloned.1.call-start = ((), (), s32[]{:S(2)}) async-start(), calls=%async_computation.5 | async-start | bytes 1966080 | tf_op jit(solution)/shard_map/reduce_scatter | solution.py:127
  1036.8 26.4 %copy-start.51 = (bf16[384,512]{1,0:T(8,128)(2,1)S(1)}, bf16[384,512]{1,0:T(8,128)(2,1)}, u32[]{:S(2)}) copy-start(bf16[384,512]{1,0:T(8,128)(2,1)} %fusion.11) | copy-start | bytes 1179652
  (73 other events, 164.7 us)
Sparse Core Ops, SparseCore 0:
  726.0 21.1 all-gather.8
  751.7 19.6 all-gather.10
  773.5 124.4 all-gather.12
  900.0 122.6 all-gather.14
  1036.9 26.2 reduce-scatter.1
where the time goes:
time: 1080 us; the launch traced here: 1070 us
  local copies, waits for them, and re-layouts  448 us (41%)
  waiting for transfers between devices  317 us (29%)
  other arithmetic  136 us (13%)
  blocking collectives  124 us (11%)
  matrix products  32 us (3%)
  between operations  15.1 us (1%)
    slice x112, local copies, waits for them, and re-layouts, local_states(): lax.associative_scan(chain_link, (decay_re, decay_im, feed_re, feed_im),...  275 us
    pad x60, local copies, waits for them, and re-layouts, local_states(): lax.associative_scan(chain_link, (decay_re, decay_im, feed_re, feed_im),...  142 us
    all_gather x1, waiting for transfers between devices, per_device(): lax.all_gather(up_weight, 'sp', axis=0, tiled=True)  125 us
    all_gather x1, waiting for transfers between devices, per_device(): lax.all_gather(down_weight, 'sp', axis=0, tiled=True)  125 us
    all_gather x4, blocking collectives, prefix(): gathered = jax.tree.map(lambda a: lax.all_gather(a, axis), part)  124 us
    add x26, other arithmetic, local_states(): lax.associative_scan(chain_link, (decay_re, decay_im, feed_re, feed_im),...  28.7 us
    add x1, other arithmetic, local_states(): feed_im = drive_re * proj_im + drive_im * proj_re  27.8 us
    reduce_scatter x1, waiting for transfers between devices, per_device(): lax.psum_scatter(partials.astype(jnp.bfloat16), 'tp', scatter_dimension=1...  26.4 us
  transfers between devices with their start and end apart: 5, of which 5 were waited for; matrix products, arithmetic and copies ran while one was open for 0% of the time, Pallas kernels for 0%

commit v1 on v0

v1 whole, which is shorter than its diff:
```python
import functools

import jax
import jax.numpy as jnp
from jax import lax
from jax.experimental import pallas as pl
from jax.experimental.pallas import tpu as pltpu
from jax.sharding import PartitionSpec as P

rms_eps = 1e-06
segments = 8
MESH = pl.DeviceIdType.MESH
f32, bf16 = jnp.float32, jnp.bfloat16


def sine_cosine(x):
    y = x * x
    s = 1.0 + y * (-1 / 6 + y * (1 / 120 + y * (-1 / 5040 + y * (1 / 362880 + y * (-1 / 39916800)))))
    c = 1.0 + y * (
        -0.5
        + y * (1 / 24 + y * (-1 / 720 + y * (1 / 40320 + y * (-1 / 3628800 + y * (1 / 479001600)))))
    )
    return x * s, c


def expm1_small(y):
    return y * (
        1.0
        + y * (1 / 2 + y * (1 / 6 + y * (1 / 24 + y * (1 / 120 + y * (1 / 720 + y * (1 / 5040))))))
    )


def kernel(
    n,
    ntp,
    resid_ref,
    mixer_ref,
    step_ref,
    rates_ref,
    w_in_ref,
    w_out_ref,
    skip_ref,
    value_ref,
    gate_ref,
    gain_ref,
    up_ref,
    down_ref,
    perm_ref,
    unperm_ref,
    out_ref,
    whole,
    dre,
    dim,
    fre,
    fim,
    step_wide,
    proj,
    ends,
    carries,
    entry,
    mixer_perm,
    mixed_perm,
    chan,
    upd,
    normed,
    hidden,
    parts,
    landed,
    ring_send,
    ring_recv,
    own_sem,
    carry_send,
    carry_recv,
    chan_send,
    chan_recv,
    upd_send,
    upd_recv,
    part_send,
    part_recv,
):
    sp = lax.axis_index("sp")
    tp = lax.axis_index("tp")
    tokens, width = mixer_ref.shape
    block = up_ref.shape[0]
    pieces = ring_send.shape[3]
    piece = block // (2 * pieces)
    chunks = w_in_ref.shape[0]
    lanes = w_in_ref.shape[2] // 2
    kin = w_in_ref.shape[1]
    length = tokens // segments

    odd = sp % 2
    pos = (1 - odd) * (sp // 2) + odd * (n - 1 - sp // 2)

    def at_pos(p):
        p = (p + 2 * n) % n
        high = p // (n // 2)
        return (1 - high) * 2 * p + high * (2 * (n - 1 - p) + 1)

    ahead, behind = at_pos(pos + 1), at_pos(pos - 1)

    barrier = pltpu.get_barrier_semaphore()
    for i in range(1, n):
        pl.semaphore_signal(barrier, inc=1, device_id=((sp + i) % n, tp), device_id_type=MESH)
    for i in range(1, ntp):
        pl.semaphore_signal(barrier, inc=1, device_id=(sp, (tp + i) % ntp), device_id_type=MESH)
    pl.semaphore_wait(barrier, n - 1 + ntp - 1)

    def rows_of(owner, way, part):
        return pl.ds(pl.multiple_of(owner * block + (way * pieces + part) * piece, piece), piece)

    def ring_copy(which, way, k, part, sending):
        source = (up_ref, down_ref)[which]
        sign = -1 if way == 0 else 1
        to = ahead if way == 0 else behind
        shift = k if sending else k + 1
        owner = at_pos(pos + sign * shift)
        slot = whole.at[which, rows_of(owner, way, part)]
        if k == 0 and sending:
            src = source.at[pl.ds((way * pieces + part) * piece, piece)]
        else:
            src = slot
        return pltpu.make_async_remote_copy(
            src_ref=src,
            dst_ref=slot,
            send_sem=ring_send.at[which, way, k, part],
            recv_sem=ring_recv.at[which, way, k, part],
            device_id=(to, tp),
            device_id_type=MESH,
        )

    def service(index):
        which, k = index // (n - 1), index % (n - 1)
        for part in range(pieces):
            for way in range(2):
                if k > 0:
                    ring_copy(which, way, k - 1, part, False).wait_recv()
                ring_copy(which, way, k, part, True).start()

    def finish(which):
        for part in range(pieces):
            for way in range(2):
                ring_copy(which, way, n - 2, part, False).wait_recv()

    queue = list(range(2 * (n - 1)))

    def serve(count=1):
        for _ in range(count):
            if queue:
                service(queue.pop(0))

    own = []
    for which, source in enumerate((up_ref, down_ref)):
        start = pl.multiple_of(sp * block, block)
        c = pltpu.make_async_copy(source, whole.at[which, pl.ds(start, block)], own_sem.at[which])
        c.start()
        own.append(c)
    serve()

    mixer_perm[...] = jnp.dot(
        perm_ref[...], mixer_ref[...], preferred_element_type=f32
    ).astype(bf16)
    step_size = jnp.exp(step_ref[...])
    groups = step_size.shape[1]
    for c in range(chunks):
        cols = pl.ds(c * lanes, lanes)
        span = lanes * chunks // groups
        spread = (
            lax.broadcasted_iota(jnp.int32, (groups, lanes), 0) * span
            - lax.broadcasted_iota(jnp.int32, (groups, lanes), 1)
            - c * lanes
        )
        spread = jnp.where((spread <= 0) & (spread > -span), 1.0, 0.0).astype(f32)
        step_wide[...] = jnp.dot(
            step_size, spread, precision=lax.Precision.HIGHEST, preferred_element_type=f32
        )
        proj[...] = jnp.dot(
            mixer_perm[:, c * kin : (c + 1) * kin], w_in_ref[c], preferred_element_type=f32
        )
        shape = (segments, lanes)
        rate = jnp.broadcast_to(rates_ref[0:1, cols], shape)
        half_angle = jnp.broadcast_to(rates_ref[1:2, cols], shape) * 0.5
        rate_n = jnp.broadcast_to(rates_ref[2:3, cols], shape)
        angle_n = jnp.broadcast_to(rates_ref[3:4, cols], shape)

        def one(j, state):
            pr, pi, sr, si = state
            rows = pl.ds(pl.multiple_of(j * segments, segments), segments)
            step = step_wide[rows, :]
            s, co = sine_cosine(half_angle * step)
            em = expm1_small(-rate * step)
            factor = 1.0 + em
            twice = 2.0 * s * s
            cos_r = 1.0 - twice
            dr = factor * cos_r
            di = factor * (2.0 * s * co)
            mr = em * cos_r - twice
            vr = di * angle_n - mr * rate_n
            vi = -di * rate_n - mr * angle_n
            a = proj[rows, 0:lanes]
            b = proj[rows, lanes : 2 * lanes]
            fr = vr * a - vi * b
            fi = vr * b + vi * a
            dre[rows, cols] = dr
            dim[rows, cols] = di
            fre[rows, cols] = fr
            fim[rows, cols] = fi
            return (
                dr * pr - di * pi,
                dr * pi + di * pr,
                dr * sr - di * si + fr,
                dr * si + di * sr + fi,
            )

        zero = jnp.zeros(shape, f32)
        last = lax.fori_loop(0, length, one, (zero + 1.0, zero, zero, zero), unroll=2)
        for i in range(4):
            ends[i, :, cols] = last[i]
        serve()

    def link(earlier, later):
        return (
            later[0] * earlier[0] - later[1] * earlier[1] + later[2],
            later[0] * earlier[1] + later[1] * earlier[0] + later[3],
        )

    pr, pi, sr, si = (ends[i, 0:1, :] for i in range(4))
    for s in range(1, segments):
        qr, qi, tr, ti = (ends[i, s : s + 1, :] for i in range(4))
        pr, pi = qr * pr - qi * pi, qr * pi + qi * pr
        sr, si = link((sr, si), (qr, qi, tr, ti))
    for i, v in enumerate((pr, pi, sr, si)):
        carries[sp, i : i + 1, :] = v

    def carry_copy(i, sending):
        there = (sp + i) % n
        slot = sp if sending else (sp + n - i) % n
        return pltpu.make_async_remote_copy(
            src_ref=carries.at[slot],
            dst_ref=carries.at[slot],
            send_sem=carry_send.at[i - 1],
            recv_sem=carry_recv.at[i - 1],
            device_id=(there, tp),
            device_id_type=MESH,
        )

    for i in range(1, n):
        carry_copy(i, True).start()
    for i in range(1, n):
        carry_copy(i, False).wait_recv()
    cr = jnp.zeros_like(pr)
    ci = jnp.zeros_like(pr)
    for d in range(n - 1):
        nr, ni = link((cr, ci), tuple(carries[d, i : i + 1, :] for i in range(4)))
        cr = jnp.where(d < sp, nr, cr)
        ci = jnp.where(d < sp, ni, ci)
    for s in range(segments):
        entry[0, s : s + 1, :] = cr
        entry[1, s : s + 1, :] = ci
        cr, ci = link((cr, ci), tuple(ends[i, s : s + 1, :] for i in range(4)))
    serve()

    for c in range(chunks):
        cols = pl.ds(c * lanes, lanes)

        def again(j, state):
            rows = pl.ds(pl.multiple_of(j * segments, segments), segments)
            dr, di = dre[rows, cols], dim[rows, cols]
            xr, xi = link(state, (dr, di, fre[rows, cols], fim[rows, cols]))
            proj[rows, 0:lanes] = xr
            proj[rows, lanes : 2 * lanes] = xi
            return xr, xi

        lax.fori_loop(0, length, again, (entry[0, :, cols], entry[1, :, cols]), unroll=4)
        ins = slice(c * kin, (c + 1) * kin)
        mech = jnp.dot(proj[...].astype(bf16), w_out_ref[c], preferred_element_type=f32)
        mech = mech + skip_ref[0:1, ins] * mixer_perm[:, ins].astype(f32)
        mixed_perm[:, ins] = jax.nn.gelu(mech).astype(bf16)
        if c % 2 == 1:
            serve()
    chan[tp] = jnp.dot(unperm_ref[...], mixed_perm[...], preferred_element_type=f32).astype(bf16)

    def tp_copy(buf, sems, i, sending):
        slot = tp if sending else (tp + ntp - i) % ntp
        return pltpu.make_async_remote_copy(
            src_ref=buf.at[slot],
            dst_ref=buf.at[slot],
            send_sem=sems[0].at[i - 1],
            recv_sem=sems[1].at[i - 1],
            device_id=(sp, (tp + i) % ntp),
            device_id_type=MESH,
        )

    chan_sems, upd_sems = (chan_send, chan_recv), (upd_send, upd_recv)
    for i in range(1, ntp):
        tp_copy(chan, chan_sems, i, True).start()
    serve()
    for i in range(1, ntp):
        tp_copy(chan, chan_sems, i, False).wait_recv()

    tile = 256

    @pl.loop(0, width // tile)
    def _(t):
        cols = pl.ds(pl.multiple_of(t * tile, tile), tile)
        v = jnp.zeros((tokens, tile), f32)
        g = jnp.zeros((tokens, tile), f32)
        for q in range(ntp):
            rows = slice(q * width, (q + 1) * width)
            v += jnp.dot(chan[q], value_ref[rows, cols], preferred_element_type=f32)
            g += jnp.dot(chan[q], gate_ref[rows, cols], preferred_element_type=f32)
        upd[tp, :, cols] = (resid_ref[:, cols].astype(f32) + v * jax.nn.sigmoid(g)).astype(bf16)

    for i in range(1, ntp):
        tp_copy(upd, upd_sems, i, True).start()
    serve()
    for i in range(1, ntp):
        tp_copy(upd, upd_sems, i, False).wait_recv()

    total = jnp.zeros((tokens, 1), f32)
    for q in range(ntp):
        u = upd[q].astype(f32)
        total += jnp.sum(u * u, axis=1, keepdims=True)
    inv = lax.rsqrt(total * (1.0 / (width * ntp)) + rms_eps)
    for q in range(ntp):
        cols = slice(q * width, (q + 1) * width)
        normed[:, cols] = (upd[q].astype(f32) * inv * gain_ref[0:1, cols]).astype(bf16)

    while queue and queue[0] < n - 1:
        serve()
    for c in own:
        c.wait()
    if queue and queue[0] == n - 1:
        serve()
    finish(0)

    @pl.loop(0, hidden.shape[1] // tile)
    def _(t):
        cols = pl.ds(pl.multiple_of(t * tile, tile), tile)
        r = jnp.dot(normed[...], whole[0, :, cols], preferred_element_type=f32)
        r = jnp.maximum(r, 0.0)
        hidden[:, cols] = (r * r).astype(bf16)

    while queue:
        serve()
    finish(1)

    per = width // tile

    def part_copy(i, sending):
        there = (tp + i) % ntp
        slot = tp if sending else (tp + ntp - i) % ntp
        return pltpu.make_async_remote_copy(
            src_ref=parts.at[i],
            dst_ref=landed.at[slot],
            send_sem=part_send.at[i - 1],
            recv_sem=part_recv.at[i - 1],
            device_id=(sp, there),
            device_id_type=MESH,
        )

    for i in (2, 1, 3, 0)[:ntp] if ntp == 4 else range(ntp - 1, -1, -1):
        there = (tp + i) % ntp

        @pl.loop(0, per)
        def _(t):
            rows = pl.ds(pl.multiple_of(there * width + t * tile, tile), tile)
            p = lax.dot_general(
                hidden[...],
                whole[1, rows, :],
                (((1,), (1,)), ((), ())),
                preferred_element_type=f32,
            )
            parts[i, t] = p.astype(bf16)

        if i > 0:
            part_copy(i, True).start()

    for i in range(1, ntp):
        part_copy(i, False).wait_recv()
    for t in range(per):
        cols = slice(t * tile, (t + 1) * tile)
        acc = parts[0, t].astype(f32)
        for i in range(1, ntp):
            acc += landed[(tp + i) % ntp, t].astype(f32)
        out_ref[:, cols] = (upd[tp, :, cols].astype(f32) + acc).astype(bf16)

    for which in range(2):
        for k in range(n - 1):
            for way in range(2):
                for part in range(pieces):
                    ring_copy(which, way, k, part, True).wait_send()
    for i in range(1, n):
        carry_copy(i, True).wait_send()
    for i in range(1, ntp):
        tp_copy(chan, chan_sems, i, True).wait_send()
        tp_copy(upd, upd_sems, i, True).wait_send()
        part_copy(i, True).wait_send()


def per_device(
    n,
    ntp,
    resid,
    mixer_in,
    log_step,
    decay_real,
    frequency,
    input_matrix,
    output_matrix,
    skip_gain,
    value_weight,
    gate_weight,
    norm_gain,
    up_weight,
    down_weight,
):
    tokens, width = mixer_in.shape
    groups, states = decay_real.shape
    per = width // groups
    bunch = min(128 // per, groups)
    chunks = groups // bunch
    kin, lanes = bunch * per, bunch * states
    features, units = value_weight.shape[0], up_weight.shape[1]
    length = tokens // segments
    modulus = decay_real * decay_real + frequency * frequency
    rates = jnp.stack(
        [decay_real, frequency, decay_real / modulus, frequency / modulus]
    ).reshape(4, groups * states)
    same = jnp.eye(bunch, dtype=bf16)
    w_in = input_matrix.astype(bf16).reshape(2, chunks, bunch, states, per)
    w_in = w_in.transpose(1, 2, 4, 0, 3)[:, :, :, :, None, :]
    w_in = (w_in * same[None, :, None, None, :, None]).reshape(chunks, kin, 2 * lanes)
    w_out = jnp.stack([output_matrix[0], -output_matrix[1]]).astype(bf16)
    w_out = w_out.reshape(2, chunks, bunch, per, states).transpose(1, 0, 2, 4, 3)
    w_out = (w_out[:, :, :, :, None, :] * same[None, None, :, None, :, None]).reshape(
        chunks, 2 * lanes, kin
    )
    step_perm = log_step.reshape(segments, length, groups).transpose(1, 0, 2)
    step_perm = step_perm.reshape(tokens, groups)
    row = jnp.arange(tokens)
    perm = (row[None, :] == ((row % segments) * length + row // segments)[:, None]).astype(bf16)
    pieces = 2
    total = groups * states
    tile = 256
    dma = pltpu.SemaphoreType.DMA
    vmem = pl.BlockSpec(memory_space=pltpu.VMEM)
    return pl.pallas_call(
        functools.partial(kernel, n, ntp),
        out_shape=jax.ShapeDtypeStruct((tokens, width), bf16),
        in_specs=[vmem] * 14,
        out_specs=vmem,
        scratch_shapes=[
            pltpu.VMEM((2, features, units), bf16),
            pltpu.VMEM((tokens, total), f32),
            pltpu.VMEM((tokens, total), f32),
            pltpu.VMEM((tokens, total), f32),
            pltpu.VMEM((tokens, total), f32),
            pltpu.VMEM((tokens, lanes), f32),
            pltpu.VMEM((tokens, 2 * lanes), f32),
            pltpu.VMEM((4, segments, total), f32),
            pltpu.VMEM((n, 4, total), f32),
            pltpu.VMEM((2, segments, total), f32),
            pltpu.VMEM((tokens, width), bf16),
            pltpu.VMEM((tokens, width), bf16),
            pltpu.VMEM((ntp, tokens, width), bf16),
            pltpu.VMEM((ntp, tokens, width), bf16),
            pltpu.VMEM((tokens, features), bf16),
            pltpu.VMEM((tokens, units), bf16),
            pltpu.VMEM((ntp, width // tile, tokens, tile), bf16),
            pltpu.VMEM((ntp, width // tile, tokens, tile), bf16),
            dma((2, 2, n - 1, pieces)),
            dma((2, 2, n - 1, pieces)),
            dma((2,)),
            dma((n - 1,)),
            dma((n - 1,)),
            dma((ntp - 1,)),
            dma((ntp - 1,)),
            dma((ntp - 1,)),
            dma((ntp - 1,)),
            dma((ntp - 1,)),
            dma((ntp - 1,)),
        ],
        compiler_params=pltpu.CompilerParams(
            collective_id=0, has_side_effects=True, vmem_limit_bytes=64 * 1024 * 1024 - 65536
        ),
    )(
        resid,
        mixer_in,
        step_perm,
        rates,
        w_in,
        w_out,
        skip_gain.reshape(1, width),
        value_weight,
        gate_weight,
        norm_gain.reshape(1, features),
        up_weight,
        down_weight,
        perm,
        perm.T,
    )


def solution(mesh):
    in_specs = (
        P("sp", "tp"),
        P("sp", "tp"),
        P("sp", "tp"),
        P("tp", None),
        P("tp", None),
        P(None, "tp", None, None),
        P(None, "tp", None, None),
        P("tp"),
        P(None, "tp"),
        P(None, "tp"),
        P(),
        P("sp", "tp"),
        P("sp", "tp"),
    )
    body = functools.partial(per_device, mesh.shape["sp"], mesh.shape["tp"])
    return jax.shard_map(
        body, mesh=mesh, in_specs=in_specs, out_specs=P("sp", "tp"), check_vma=False
    )
```

time: 1080 us -> 212 us (0.20)
  local copies, waits for them, and re-layouts: 448 us -> 11.5 us
  waiting for transfers between devices: 317 us -> 0 us
  Pallas kernels: 0 us -> 194 us
  other arithmetic: 136 us -> 5.69 us
  blocking collectives: 124 us -> 0 us
  matrix products: 32 us -> 0 us
  between operations: 15.1 us -> 0.16 us
    all_gather x4 -> x0, waiting for transfers between devices: 289 us -> none  [the longest x1 125 us: per_device(): lax.all_gather(up_weight, 'sp', axis=0, tiled=True)]
    slice x112 -> x1, local copies, waits for them, and re-layouts: 275 us -> 0.02 us  [per_device(): w_out = jnp.stack([output_matrix[0], -output_matrix[1]]).astype(bf16)]
    pallas_call x0 -> x1, Pallas kernels: none -> 194 us  [per_device(): pl.pallas_call(functools.partial(kernel, n, ntp), out_shape=jax.ShapeDtyp...]
    pad x60 -> x0, local copies, waits for them, and re-layouts: 142 us -> none  [local_states(): lax.associative_scan(chain_link, (decay_re, decay_im, feed_re, feed_im),...]
    all_gather x4 -> x0, blocking collectives: 124 us -> none  [prefix(): gathered = jax.tree.map(lambda a: lax.all_gather(a, axis), part)]
    add x49 -> x1, other arithmetic: 92.8 us -> 0.01 us  [per_device(): row % segments * length + row // segments]
    dot_general x7 -> x0, matrix products: 32 us -> none  [the longest x1 14.1 us: per_device(): lax.dot_general(hidden, lax.all_gather(down_weight, 'sp', axis=0, tiled=T...]
    reduce_scatter x1 -> x0, waiting for transfers between devices: 26.4 us -> none  [per_device(): lax.psum_scatter(partials.astype(jnp.bfloat16), 'tp', scatter_dimension=1...]
  transfers between devices with their start and end apart: 5 -> 0, of which waited for: 5 -> 0; matrix products, arithmetic and copies ran while one was open for 0% -> 0% of each run, Pallas kernels for 0% -> 0%
where the time goes in v1:
time: 212 us
  Pallas kernels  194 us (92%)
  local copies, waits for them, and re-layouts  11.5 us (5%)
  other arithmetic  5.69 us (3%)
    pallas_call x1, Pallas kernels, per_device(): pl.pallas_call(functools.partial(kernel, n, ntp), out_shape=jax.ShapeDtyp...  194 us

profile of v1, /device:TPU:0, one launch (start us, length us, event | category | flops | bytes accessed | tf_op | source)
XLA Modules:
  0.0 211.5 jit_solution(9064603671024038357)
XLA Ops:
  0.0 0.9 reshape.75
  0.9 0.8 copy.17
  1.7 0.7 fusion.3
  2.5 0.1 stack.26
  2.5 0.1 stack.25
  2.6 0.8 stack.24
  3.4 0.8 stack.23
  4.2 0.6 pad_maximum_fusion.rates_ref
  4.9 1.1 convert_element_type.23
  5.9 0.3 copy.18
  6.2 0.6 mul.60
  6.8 1.5 mul.61
  8.3 0.0 copy-start
  8.3 0.1 copy.19
  8.4 0.1 mul.62
  8.5 0.3 mul.63
  8.9 1.1 broadcast_multiply_fusion.1.w_in_ref
  10.0 0.0 copy-done
  10.0 0.1 maximum_bitcast_fusion
  10.1 0.1 copy.20
  10.2 0.5 mul.66
  10.6 1.5 mul.67
  12.1 0.7 copy.22
  12.8 0.1 mul.68
  12.9 0.3 mul.69
  13.3 0.2 copy.21
  13.5 1.1 broadcast_multiply_fusion.w_out_ref
  14.6 0.9 fusion.1
  15.5 194.2 %shard_map.127 = bf16[384,512]{1,0:T(8,128)(2,1)} custom-call(bf16[384,512]{1,0:T(8,128)(2,1)} %resid_ref.1, bf16[384,512]{1,0:T(8,128)(2,1)} %mixer_ref.1, f32[384,32]{1,0:T(8,128)} %bitcast.27, f32[4,2048]{1,0:T(4,128)} %pad_maximum_fusion.rates_ref, bf16[4,128,1024]{2,1,0:T(8,128)(2,1)} %broadcast_multiply_fusion.1.w_in_ref, ...), custom_call_target="tpu_custom_call" | custom-call | tf_op jit(solution)/shard_map/pallas_call | solution.py:448
  209.8 1.8 copy.24
  (4 shorter events, 0.1 us)
Async XLA Ops:
  8.3 1.7 copy-start

commit v2 on v1

--- a/solution.py
+++ b/solution.py
@@ -2,6 +2,7 @@
 
 import jax
 import jax.numpy as jnp
+import numpy as np
 from jax import lax
 from jax.experimental import pallas as pl
 from jax.experimental.pallas import tpu as pltpu
@@ -36,7 +37,8 @@
     resid_ref,
     mixer_ref,
     step_ref,
-    rates_ref,
+    decay_ref,
+    angle_ref,
     w_in_ref,
     w_out_ref,
     skip_ref,
@@ -84,9 +86,11 @@
     block = up_ref.shape[0]
     pieces = ring_send.shape[3]
     piece = block // (2 * pieces)
-    chunks = w_in_ref.shape[0]
-    lanes = w_in_ref.shape[2] // 2
-    kin = w_in_ref.shape[1]
+    groups, states = decay_ref.shape
+    each = width // groups
+    bunch = min(128 // each, groups)
+    chunks = groups // bunch
+    lanes, kin = bunch * states, bunch * each
     length = tokens // segments
 
     odd = sp % 2
@@ -160,28 +164,75 @@
     mixer_perm[...] = jnp.dot(
         perm_ref[...], mixer_ref[...], preferred_element_type=f32
     ).astype(bf16)
-    step_size = jnp.exp(step_ref[...])
-    groups = step_size.shape[1]
+    highest = lax.Precision.HIGHEST
+    step_size = jnp.dot(
+        perm_ref[...].astype(f32),
+        jnp.exp(step_ref[...]),
+        precision=highest,
+        preferred_element_type=f32,
+    )
+
+    def iota(shape, axis):
+        return lax.broadcasted_iota(jnp.int32, shape, axis)
+
+    def ones_where(mask, dtype=f32):
+        return jnp.where(mask, 1.0, 0.0).astype(dtype)
+
+    def belongs(rows, columns, span, first):
+        gap = iota((rows, columns), 1) + first - iota((rows, columns), 0) * span
+        return ones_where((gap >= 0) & (gap < span))
+
+    def tiled(size, copies):
+        shape = (size, size * copies)
+        hits = jnp.zeros(shape, f32)
+        for i in range(copies):
+            hits += ones_where(iota(shape, 1) - iota(shape, 0) == i * size)
+        return hits
+
+    over_states = tiled(states, bunch)
+    over_each = tiled(each, bunch).astype(bf16)
+    agree = jnp.zeros((kin, lanes), f32)
+    agree_t = jnp.zeros((lanes, kin), f32)
+    for i in range(bunch):
+        r, l = iota((kin, lanes), 0) - i * each, iota((kin, lanes), 1) - i * states
+        agree += ones_where((r >= 0) & (r < each) & (l >= 0) & (l < states))
+        r, l = iota((lanes, kin), 1) - i * each, iota((lanes, kin), 0) - i * states
+        agree_t += ones_where((r >= 0) & (r < each) & (l >= 0) & (l < states))
+
+    def wide_rate(table, c):
+        spread = jnp.dot(table, over_states, precision=highest, preferred_element_type=f32)
+        return jnp.sum(
+            spread * belongs(groups, lanes, states, c * lanes), axis=0, keepdims=True
+        )
+
     for c in range(chunks):
         cols = pl.ds(c * lanes, lanes)
-        span = lanes * chunks // groups
-        spread = (
-            lax.broadcasted_iota(jnp.int32, (groups, lanes), 0) * span
-            - lax.broadcasted_iota(jnp.int32, (groups, lanes), 1)
-            - c * lanes
-        )
-        spread = jnp.where((spread <= 0) & (spread > -span), 1.0, 0.0).astype(f32)
         step_wide[...] = jnp.dot(
-            step_size, spread, precision=lax.Precision.HIGHEST, preferred_element_type=f32
-        )
-        proj[...] = jnp.dot(
-            mixer_perm[:, c * kin : (c + 1) * kin], w_in_ref[c], preferred_element_type=f32
-        )
+            step_size,
+            belongs(groups, lanes, states, c * lanes),
+            precision=highest,
+            preferred_element_type=f32,
+        )
+        for i in range(2):
+            matrix = jnp.dot(
+                w_in_ref[i, c * lanes : (c + 1) * lanes, :].astype(bf16),
+                over_each,
+                preferred_element_type=f32,
+            )
+            proj[:, i * lanes : (i + 1) * lanes] = lax.dot_general(
+                mixer_perm[:, c * kin : (c + 1) * kin],
+                (matrix * agree_t).astype(bf16),
+                (((1,), (1,)), ((), ())),
+                preferred_element_type=f32,
+            )
+        rate_row = wide_rate(decay_ref[...], c)
+        angle_row = wide_rate(angle_ref[...], c)
+        modulus = rate_row * rate_row + angle_row * angle_row
         shape = (segments, lanes)
-        rate = jnp.broadcast_to(rates_ref[0:1, cols], shape)
-        half_angle = jnp.broadcast_to(rates_ref[1:2, cols], shape) * 0.5
-        rate_n = jnp.broadcast_to(rates_ref[2:3, cols], shape)
-        angle_n = jnp.broadcast_to(rates_ref[3:4, cols], shape)
+        rate = jnp.broadcast_to(rate_row, shape)
+        half_angle = jnp.broadcast_to(angle_row * 0.5, shape)
+        rate_n = jnp.broadcast_to(rate_row / modulus, shape)
+        angle_n = jnp.broadcast_to(angle_row / modulus, shape)
 
         def one(j, state):
             pr, pi, sr, si = state
@@ -273,7 +324,19 @@
 
         lax.fori_loop(0, length, again, (entry[0, :, cols], entry[1, :, cols]), unroll=4)
         ins = slice(c * kin, (c + 1) * kin)
-        mech = jnp.dot(proj[...].astype(bf16), w_out_ref[c], preferred_element_type=f32)
+        mech = jnp.zeros((tokens, kin), f32)
+        for i in range(2):
+            matrix = jnp.dot(
+                w_out_ref[i, c * kin : (c + 1) * kin, :].astype(bf16),
+                over_states.astype(bf16),
+                preferred_element_type=f32,
+            )
+            mech += (1 - 2 * i) * lax.dot_general(
+                proj[:, i * lanes : (i + 1) * lanes].astype(bf16),
+                (matrix * agree).astype(bf16),
+                (((1,), (1,)), ((), ())),
+                preferred_element_type=f32,
+            )
         mech = mech + skip_ref[0:1, ins] * mixer_perm[:, ins].astype(f32)
         mixed_perm[:, ins] = jax.nn.gelu(mech).astype(bf16)
         if c % 2 == 1:
@@ -341,46 +404,59 @@
         r = jnp.maximum(r, 0.0)
         hidden[:, cols] = (r * r).astype(bf16)
 
-    while queue:
-        serve()
-    finish(1)
-
-    per = width // tile
-
-    def part_copy(i, sending):
+    per = 2 * n // ntp
+    half = block // 2
+
+    def part_copy(h):
+        return pltpu.make_async_remote_copy(
+            src_ref=parts.at[h],
+            dst_ref=landed.at[tp, h % per],
+            send_sem=part_send.at[h],
+            recv_sem=part_recv.at[tp, h % per],
+            device_id=(sp, h // per),
+            device_id_type=MESH,
+        )
+
+    def down_part(owner, way):
+        h = 2 * owner + way
+        rows = pl.ds(pl.multiple_of(h * half, half), half)
+        p = lax.dot_general(
+            hidden[...],
+            whole[1, rows, :],
+            (((1,), (1,)), ((), ())),
+            preferred_element_type=f32,
+        )
+        parts[h] = p.astype(bf16)
+
+        @pl.when(h // per != tp)
+        def _():
+            part_copy(h).start()
+
+    down_part(sp, 0)
+    down_part(sp, 1)
+    for k in range(n - 1):
+        if k < n - 2:
+            while queue and queue[0] <= n + k:
+                serve()
+        else:
+            finish(1)
+        down_part(at_pos(pos - k - 1), 0)
+        down_part(at_pos(pos + k + 1), 1)
+
+    for i in range(1, ntp):
         there = (tp + i) % ntp
-        slot = tp if sending else (tp + ntp - i) % ntp
-        return pltpu.make_async_remote_copy(
-            src_ref=parts.at[i],
-            dst_ref=landed.at[slot],
-            send_sem=part_send.at[i - 1],
-            recv_sem=part_recv.at[i - 1],
-            device_id=(sp, there),
-            device_id_type=MESH,
-        )
-
-    for i in (2, 1, 3, 0)[:ntp] if ntp == 4 else range(ntp - 1, -1, -1):
-        there = (tp + i) % ntp
-
-        @pl.loop(0, per)
-        def _(t):
-            rows = pl.ds(pl.multiple_of(there * width + t * tile, tile), tile)
-            p = lax.dot_general(
-                hidden[...],
-                whole[1, rows, :],
-                (((1,), (1,)), ((), ())),
-                preferred_element_type=f32,
-            )
-            parts[i, t] = p.astype(bf16)
-
-        if i > 0:
-            part_copy(i, True).start()
-
-    for i in range(1, ntp):
-        part_copy(i, False).wait_recv()
+        for t in range(per):
+            pltpu.make_async_remote_copy(
+                src_ref=parts.at[t],
+                dst_ref=landed.at[there, t],
+                send_sem=part_send.at[t],
+                recv_sem=part_recv.at[there, t],
+                device_id=(sp, there),
+                device_id_type=MESH,
+            ).wait_recv()
     for t in range(per):
-        cols = slice(t * tile, (t + 1) * tile)
-        acc = parts[0, t].astype(f32)
+        cols = slice(t * half, (t + 1) * half)
+        acc = parts[tp * per + t].astype(f32)
         for i in range(1, ntp):
             acc += landed[(tp + i) % ntp, t].astype(f32)
         out_ref[:, cols] = (upd[tp, :, cols].astype(f32) + acc).astype(bf16)
@@ -395,7 +471,11 @@
     for i in range(1, ntp):
         tp_copy(chan, chan_sems, i, True).wait_send()
         tp_copy(upd, upd_sems, i, True).wait_send()
-        part_copy(i, True).wait_send()
+    for h in range(2 * n):
+
+        @pl.when(h // per != tp)
+        def _():
+            part_copy(h).wait_send()
 
 
 def per_device(
@@ -423,32 +503,16 @@
     kin, lanes = bunch * per, bunch * states
     features, units = value_weight.shape[0], up_weight.shape[1]
     length = tokens // segments
-    modulus = decay_real * decay_real + frequency * frequency
-    rates = jnp.stack(
-        [decay_real, frequency, decay_real / modulus, frequency / modulus]
-    ).reshape(4, groups * states)
-    same = jnp.eye(bunch, dtype=bf16)
-    w_in = input_matrix.astype(bf16).reshape(2, chunks, bunch, states, per)
-    w_in = w_in.transpose(1, 2, 4, 0, 3)[:, :, :, :, None, :]
-    w_in = (w_in * same[None, :, None, None, :, None]).reshape(chunks, kin, 2 * lanes)
-    w_out = jnp.stack([output_matrix[0], -output_matrix[1]]).astype(bf16)
-    w_out = w_out.reshape(2, chunks, bunch, per, states).transpose(1, 0, 2, 4, 3)
-    w_out = (w_out[:, :, :, :, None, :] * same[None, None, :, None, :, None]).reshape(
-        chunks, 2 * lanes, kin
-    )
-    step_perm = log_step.reshape(segments, length, groups).transpose(1, 0, 2)
-    step_perm = step_perm.reshape(tokens, groups)
-    row = jnp.arange(tokens)
-    perm = (row[None, :] == ((row % segments) * length + row // segments)[:, None]).astype(bf16)
+    row = np.arange(tokens)
+    perm = (row[None, :] == ((row % segments) * length + row // segments)[:, None]).astype(np.float32)
     pieces = 2
     total = groups * states
-    tile = 256
     dma = pltpu.SemaphoreType.DMA
     vmem = pl.BlockSpec(memory_space=pltpu.VMEM)
     return pl.pallas_call(
         functools.partial(kernel, n, ntp),
         out_shape=jax.ShapeDtypeStruct((tokens, width), bf16),
-        in_specs=[vmem] * 14,
+        in_specs=[vmem] * 15,
         out_specs=vmem,
         scratch_shapes=[
             pltpu.VMEM((2, features, units), bf16),
@@ -467,8 +531,8 @@
             pltpu.VMEM((ntp, tokens, width), bf16),
             pltpu.VMEM((tokens, features), bf16),
             pltpu.VMEM((tokens, units), bf16),
-            pltpu.VMEM((ntp, width // tile, tokens, tile), bf16),
-            pltpu.VMEM((ntp, width // tile, tokens, tile), bf16),
+            pltpu.VMEM((2 * n, tokens, features // (2 * n)), bf16),
+            pltpu.VMEM((ntp, 2 * n // ntp, tokens, features // (2 * n)), bf16),
             dma((2, 2, n - 1, pieces)),
             dma((2, 2, n - 1, pieces)),
             dma((2,)),
@@ -478,8 +542,8 @@
             dma((ntp - 1,)),
             dma((ntp - 1,)),
             dma((ntp - 1,)),
-            dma((ntp - 1,)),
-            dma((ntp - 1,)),
+            dma((2 * n,)),
+            dma((ntp, 2 * n // ntp)),
         ],
         compiler_params=pltpu.CompilerParams(
             collective_id=0, has_side_effects=True, vmem_limit_bytes=64 * 1024 * 1024 - 65536
@@ -487,18 +551,19 @@
     )(
         resid,
         mixer_in,
-        step_perm,
-        rates,
-        w_in,
-        w_out,
+        log_step,
+        decay_real,
+        frequency,
+        input_matrix.reshape(2, groups * states, per),
+        output_matrix.reshape(2, groups * per, states),
         skip_gain.reshape(1, width),
         value_weight,
         gate_weight,
         norm_gain.reshape(1, features),
         up_weight,
         down_weight,
-        perm,
-        perm.T,
+        jnp.asarray(perm, bf16),
+        jnp.asarray(perm.T, bf16),
     )
 
 

time: 212 us -> 195 us (0.920)
  Pallas kernels: 194 us -> 188 us
  other arithmetic: 5.69 us -> 0 us
  local copies, waits for them, and re-layouts: 11.5 us -> 6.39 us
    pallas_call x1, Pallas kernels: 194 us -> 188 us  [per_device(): pl.pallas_call(functools.partial(kernel, n, ntp), out_shape=jax.ShapeDtyp...]
    mul x10 -> x0, local copies, waits for them, and re-layouts: 5.78 us -> none  [the longest x6 3.25 us: per_device(): w_out[:, :, :, :, None, :] * same[None, None, :, None, :, None]]
    unnamed x3, local copies, waits for them, and re-layouts: 1.77 us -> 6.39 us
    mul x2 -> x0, other arithmetic: 2.19 us -> none  [the longest x1 1.12 us: per_device(): w_out[:, :, :, :, None, :] * same[None, None, :, None, :, None]]
where the time goes in v2:
time: 195 us
  Pallas kernels  188 us (96%)
  local copies, waits for them, and re-layouts  6.39 us (3%)
    pallas_call x1, Pallas kernels, per_device(): pl.pallas_call(functools.partial(kernel, n, ntp), out_shape=jax.ShapeDtyp...  188 us
    unnamed x3, local copies, waits for them, and re-layouts  6.39 us

profile of v2, /device:TPU:0, one launch (start us, length us, event | category | flops | bytes accessed | tf_op | source)
XLA Modules:
  0.0 194.8 jit_solution(1021809575680240563)
XLA Ops:
  0.0 1.6 copy.17.step_ref
  1.6 3.0 %copy.16 = f32[2,32,64,16]{3,2,1,0:T(8,128)} copy(f32[2,32,64,16]{2,3,1,0:T(8,128)} %param.20) | data formatting | bytes 524288 | tf_op args[5]
  4.6 188.4 %shard_map.145 = bf16[384,512]{1,0:T(8,128)(2,1)} custom-call(bf16[384,512]{1,0:T(8,128)(2,1)} %resid_ref.1, bf16[384,512]{1,0:T(8,128)(2,1)} %mixer_ref.1, f32[384,32]{1,0:T(8,128)} %copy.17.step_ref, f32[32,64]{1,0:T(8,128)} %decay_ref.1, f32[32,64]{1,0:T(8,128)} %angle_ref.1, f32[2,2048,16]{2,1,0:T(8,128)} %bitcast.4, f32[2,512,64]{2,1,0:T(8,128)} %bitcast.5, ...), custom_call_target="tpu_custom_call" | custom-call | tf_op jit(solution)/shard_map/pallas_call | solution.py:512
  193.0 1.8 copy.19
